TPU v7x, 32 devices: a whole 2x2x4 slice. The times are simulated.
32 devices in a mesh: grp: 2 (over y), fs: 4 (over z), tp: 4 (over x, core).
Axes of the slice: x: 2, y: 2, z: 4, core: 2. Of those that a mesh axis runs over, the one named last changes fastest.
Arguments:
- tokens: bfloat16 [4096, 2048], P(('grp', 'fs')), parts along dimension 0, may hold values from -6 to 6
- pre_gain: float32 [2048], replicated, may hold values from 0.1 to 1.9
- gate_weight: float32 [2048, 5632], P('fs', 'tp'), may hold values from -0.125 to 0.125
- gate_scale: float32 [5632], P('tp'), may hold values from 0.5 to 2
- up_weight: float32 [2048, 5632], P('fs', 'tp'), may hold values from -0.125 to 0.125
- up_scale: float32 [5632], P('tp'), may hold values from 0.5 to 2
- down_weight: float32 [5632, 2048], P('tp', 'fs'), may hold values from -0.078125 to 0.078125
- down_scale: float32 [2048], replicated, may hold values from 0.3 to 3
- post_gain: float32 [2048], replicated, may hold values from 0.1 to 1.9
Outputs:
- mixed: bfloat16 [4096, 2048], P(('grp', 'fs')), parts along dimension 0
There are 2 independent parts, one for each index of `grp`. A program takes and returns all parts, laid end to end along the dimension named above; an argument that names none is the same for every part. Nothing has to cross between parts.
All inputs are finite; a program needn't handle non-finite values.
Results may differ from a plain program's by a relative error of at most 0.018.
Values may be sent and summed in bfloat16 or wider, within the bound.
A program may use at most 64 MiB of HBM per device.

v0:
```python
import jax
import jax.numpy as jnp
from jax import lax
from jax.sharding import PartitionSpec as P

EPS = 1e-06


def finish(summed, down_scale, post_gain):
    branch = summed * down_scale
    return (
        branch * lax.rsqrt(jnp.mean(branch * branch, axis=-1, keepdims=True) + EPS) * post_gain
    ).astype(jnp.bfloat16)


def body(
    tokens,
    pre_gain,
    gate_weight,
    gate_scale,
    up_weight,
    up_scale,
    down_weight,
    down_scale,
    post_gain,
):
    rows = tokens.astype(jnp.float32)
    normed = (
        rows * lax.rsqrt(jnp.mean(rows * rows, axis=-1, keepdims=True) + EPS) * pre_gain
    ).astype(jnp.bfloat16)
    gate_low = gate_weight.astype(jnp.bfloat16)
    up_low = up_weight.astype(jnp.bfloat16)
    down_low = down_weight.astype(jnp.bfloat16)
    gate_full, up_full = (
        lax.all_gather(gate_low, "fs", axis=0, tiled=True),
        lax.all_gather(up_low, "fs", axis=0, tiled=True),
    )
    gate = jnp.dot(normed, gate_full, preferred_element_type=jnp.float32) * gate_scale
    up = jnp.dot(normed, up_full, preferred_element_type=jnp.float32) * up_scale
    hidden = (jax.nn.silu(gate) * up).astype(jnp.bfloat16)
    down_full = lax.all_gather(down_low, "fs", axis=1, tiled=True)
    partial_value = jnp.dot(hidden, down_full, preferred_element_type=jnp.float32)
    summed = lax.psum(partial_value.astype(jnp.bfloat16), "tp").astype(jnp.float32)
    return finish(summed, down_scale, post_gain)


def solution(mesh):
    in_specs = (
        P(("grp", "fs"), None),
        P(),
        P("fs", "tp"),
        P("tp"),
        P("fs", "tp"),
        P("tp"),
        P("tp", "fs"),
        P(),
        P(),
    )
    out_specs = P(("grp", "fs"), None)
    return jax.shard_map(body, mesh=mesh, in_specs=in_specs, out_specs=out_specs, check_vma=False)
```

profile of v0, /device:TPU:0, one launch (start us, length us, event | category | flops | bytes accessed | tf_op | source)
XLA Modules:
  0.0 406.5 jit_solution(4546783857032367066)
XLA Ops:
  6.5 0.0 copy-start.1
  6.5 0.0 all-gather.4.cloned.1.call-start
  6.5 3.2 convert_element_type.29
  9.8 0.0 all-gather.4.cloned.1.call-update
  9.8 0.0 all-gather.6.cloned.1.call-start
  9.9 0.0 copy-done.1
  9.9 1.3 convert_element_type.30
  11.1 0.0 all-gather.6.cloned.1.call-update
  11.2 0.0 copy-start.2
  11.2 0.0 copy-start.5
  11.2 0.0 copy-start.6
  11.2 0.0 all-gather.8.cloned.1.call-start
  11.2 3.2 convert_element_type.32
  14.5 0.0 all-gather.8.cloned.1.call-update
  14.5 0.0 all-reduce.2.cloned.1.call-start
  14.5 0.0 copy-done.2
  14.6 0.5 fusion
  15.0 0.0 copy-start.7
  15.1 104.3 %all-gather.4.cloned.1.call-done = bf16[2048,1408]{1,0:T(8,128)(2,1)} async-done(((bf16[512,1408]{1,0:T(8,128)(2,1)}), bf16[2048,1408]{1,0:T(8,128)(2,1)}) %all-gather.4.cloned.1.call-update) | async-done | bytes 5767184 | tf_op jit(solution)/shard_map/all_gather | solution.py:35
  119.4 0.0 copy-done.5
  119.4 0.0 copy-done.6
  119.4 7.6 %convolution_multiply_fusion.1 = f32[512,1408]{1,0:T(8,128)} fusion(bf16[2048,1408]{1,0:T(8,128)(2,1)} %all-gather.4.cloned.1.call-done, f32[1408]{0:T(1024)S(1)} %copy-done.5, bf16[512,2048]{1,0:T(8,128)(2,1)S(1)} %copy-done.2, f32[2048]{0:T(1024)S(1)} %copy-done.6, f32[512]{0:T(512)S(1)} %add_rsqrt_fusion.1), kind=kOutput, calls=%fused_computation.10 | convolution fusion | flops 2957705216 | bytes 10763776 | tf_op jit(solution)/shard_map/dot_general | solution.py:38
  127.0 0.0 copy-start.3
  127.0 98.9 %all-gather.6.cloned.1.call-done = bf16[2048,1408]{1,0:T(8,128)(2,1)} async-done(((bf16[512,1408]{1,0:T(8,128)(2,1)}), bf16[2048,1408]{1,0:T(8,128)(2,1)}) %all-gather.6.cloned.1.call-update) | async-done | bytes 5767184 | tf_op jit(solution)/shard_map/all_gather | solution.py:36
  225.9 106.5 %all-gather.8.cloned.1.call-done = bf16[1408,2048]{1,0:T(8,128)(2,1)} async-done(((bf16[1408,512]{1,0:T(8,128)(2,1)}), bf16[1408,2048]{1,0:T(8,128)(2,1)}) %all-gather.8.cloned.1.call-update) | async-done | bytes 5767184 | tf_op jit(solution)/shard_map/all_gather | solution.py:41
  332.5 0.0 copy-done.7
  332.5 13.3 %convolution_convert_fusion = bf16[512,2048]{1,0:T(8,128)(2,1)} fusion(bf16[1408,2048]{1,0:T(8,128)(2,1)} %all-gather.8.cloned.1.call-done, bf16[2048,1408]{1,0:T(8,128)(2,1)} %all-gather.6.cloned.1.call-done, f32[512,1408]{1,0:T(8,128)} %convolution_multiply_fusion.1, f32[1408]{0:T(1024)S(1)} %copy-done.7, bf16[512,2048]{1,0:T(8,128)(2,1)S(1)} %copy-done.2, ...), kind=kOutput, calls=%fused_computation.12 | convolution fusion | flops 5915869184 | bytes 18628096 | tf_op jit(solution)/shard_map/dot_general | solution.py:42
  345.8 0.0 copy-start.4
  345.8 0.0 all-reduce.2.cloned.1.call-update
  345.8 49.8 %all-reduce.2.cloned.1.call-done = bf16[512,2048]{1,0:T(8,128)(2,1)} async-done(((bf16[512,2048]{1,0:T(8,128)(2,1)}), bf16[512,2048]{1,0:T(8,128)(2,1)}) %all-reduce.2.cloned.1.call-update) | async-done | bytes 2097168 | tf_op jit(solution)/shard_map/psum | solution.py:43
  395.6 0.0 copy-done.3
  395.6 0.0 copy-start
  395.6 2.4 multiply_reduce_fusion
  398.0 0.0 copy-done.4
  398.0 0.0 copy-done
  398.0 2.0 multiply_convert_fusion
  (2 shorter events, 0.0 us)
Async XLA Ops:
  6.5 3.3 copy-start.1
  6.5 112.8 %all-gather.4.cloned.1.call-start = ((), (), s32[]{:S(2)}) async-start(), calls=%async_computation | async-start | bytes 7208960 | tf_op jit(solution)/shard_map/all_gather | solution.py:35
  9.8 216.1 %all-gather.6.cloned.1.call-start = ((), (), s32[]{:S(2)}) async-start(), calls=%async_computation.1 | async-start | bytes 7208960 | tf_op jit(solution)/shard_map/all_gather | solution.py:36
  11.2 3.4 copy-start.2
  11.2 108.2 %copy-start.5 = (f32[1408]{0:T(1024)S(1)}, f32[1408]{0:T(1024)}, u32[]{:S(2)}) copy-start(f32[1408]{0:T(1024)} %param.12) | copy-start | bytes 16900
  11.2 108.2 %copy-start.6 = (f32[2048]{0:T(1024)S(1)}, f32[2048]{0:T(1024)}, u32[]{:S(2)}) copy-start(f32[2048]{0:T(1024)} %param.10) | copy-start | bytes 24580
  11.2 321.3 %all-gather.8.cloned.1.call-start = ((), (), s32[]{:S(2)}) async-start(), calls=%async_computation.2 | async-start | bytes 7208960 | tf_op jit(solution)/shard_map/all_gather | solution.py:41
  14.5 381.1 %all-reduce.2.cloned.1.call-start = ((), (), s32[]{:S(2)}) async-start(), calls=%async_computation.3 | async-start | bytes 4194304 | tf_op jit(solution)/shard_map/psum | solution.py:43
  15.0 317.4 %copy-start.7 = (f32[1408]{0:T(1024)S(1)}, f32[1408]{0:T(1024)}, u32[]{:S(2)}) copy-start(f32[1408]{0:T(1024)} %param.14) | copy-start | bytes 16900
  127.0 268.6 %copy-start.3 = (f32[2048]{0:T(1024)S(1)}, f32[2048]{0:T(1024)}, u32[]{:S(2)}) copy-start(f32[2048]{0:T(1024)} %param.16) | copy-start | bytes 24580
  345.8 52.2 %copy-start.4 = (f32[2048]{0:T(1024)S(1)}, f32[2048]{0:T(1024)}, u32[]{:S(2)}) copy-start(f32[2048]{0:T(1024)} %param.17) | copy-start | bytes 24580
  395.6 2.4 copy-start
Sparse Core Ops, SparseCore 0:
  9.9 109.3 all-gather.3
  120.9 104.9 all-gather.5
  227.5 104.9 all-gather.7
  345.9 49.6 all-reduce.1
where the time goes:
time: 407 us; the launch traced here: 406 us
  waiting for transfers between devices  360 us (88%)
  matrix products  21 us (5%)
  between operations  13.2 us (3%)
  other arithmetic  12.6 us (3%)
    all_gather x1, waiting for transfers between devices, body(): down_full = lax.all_gather(down_low, 'fs', axis=1, tiled=True)  107 us
    all_gather x1, waiting for transfers between devices, body(): lax.all_gather(gate_low, 'fs', axis=0, tiled=True)  104 us
    all_gather x1, waiting for transfers between devices, body(): lax.all_gather(up_low, 'fs', axis=0, tiled=True)  98.9 us
    psum x1, waiting for transfers between devices, body(): lax.psum(partial_value.astype(jnp.bfloat16), 'tp').astype(jnp.float32)  49.8 us
    dot_general x1, matrix products, body(): jnp.dot(hidden, down_full, preferred_element_type=jnp.float32)  13.3 us
  transfers between devices with their start and end apart: 4, of which 4 were waited for; matrix products, arithmetic and copies ran while one was open for 3% of the time, Pallas kernels for 0%

commit v1 on v0

--- a/solution.py
+++ b/solution.py
@@ -38,7 +38,12 @@
     gate = jnp.dot(normed, gate_full, preferred_element_type=jnp.float32) * gate_scale
     up = jnp.dot(normed, up_full, preferred_element_type=jnp.float32) * up_scale
     hidden = (jax.nn.silu(gate) * up).astype(jnp.bfloat16)
-    down_full = lax.all_gather(down_low, "fs", axis=1, tiled=True)
+    ring = [down_low]
+    for hop in range(3):
+        ring.append(lax.ppermute(ring[-1], "fs", [(dev, (dev + 1) % 4) for dev in range(4)]))
+    down_full = jnp.roll(
+        jnp.concatenate(ring[::-1], axis=1), (lax.axis_index("fs") + 1) * ring[0].shape[1], axis=1
+    )
     partial_value = jnp.dot(hidden, down_full, preferred_element_type=jnp.float32)
     summed = lax.psum(partial_value.astype(jnp.bfloat16), "tp").astype(jnp.float32)
     return finish(summed, down_scale, post_gain)

time: 407 us -> 377 us (0.926)
  waiting for transfers between devices: 360 us -> 272 us
  starting transfers between devices: 0.13 us -> 37.3 us
  local copies, waits for them, and re-layouts: 0.04 us -> 14.3 us
  other arithmetic: 12.6 us -> 17.1 us
    ppermute x0 -> x3, waiting for transfers between devices: none -> 174 us  [body(): lax.ppermute(ring[-1], 'fs', [(dev, (dev + 1) % 4) for dev in range(4)])]
    all_gather x1 -> x0, waiting for transfers between devices: 107 us -> none  [body(): down_full = lax.all_gather(down_low, 'fs', axis=1, tiled=True)]
    all_gather x1, waiting for transfers between devices: 104 us -> 0.01 us  [body(): lax.all_gather(gate_low, 'fs', axis=0, tiled=True)]
    all_gather x1, waiting for transfers between devices: 98.9 us -> 48 us  [body(): lax.all_gather(up_low, 'fs', axis=0, tiled=True)]
    ppermute x0 -> x3, starting transfers between devices: none -> 37.2 us  [body(): lax.ppermute(ring[-1], 'fs', [(dev, (dev + 1) % 4) for dev in range(4)])]
    unnamed x16 -> x24, local copies, waits for them, and re-layouts: 0.04 us -> 14.3 us
  transfers between devices with their start and end apart: 4 -> 6, of which waited for: 4 -> 5; matrix products, arithmetic and copies ran while one was open for 3% -> 8% of each run, Pallas kernels for 0% -> 0%
where the time goes in v1:
time: 377 us; the launch traced here: 376 us
  waiting for transfers between devices  272 us (72%)
  starting transfers between devices  37.3 us (10%)
  matrix products  21.9 us (6%)
  other arithmetic  17.1 us (5%)
  local copies, waits for them, and re-layouts  14.3 us (4%)
  between operations  13.2 us (4%)
    ppermute x3, waiting for transfers between devices, body(): lax.ppermute(ring[-1], 'fs', [(dev, (dev + 1) % 4) for dev in range(4)])  174 us
    psum x1, waiting for transfers between devices, body(): lax.psum(partial_value.astype(jnp.bfloat16), 'tp').astype(jnp.float32)  50.5 us
    all_gather x1, waiting for transfers between devices, body(): lax.all_gather(up_low, 'fs', axis=0, tiled=True)  48 us
    ppermute x3, starting transfers between devices, body(): lax.ppermute(ring[-1], 'fs', [(dev, (dev + 1) % 4) for dev in range(4)])  37.2 us
    unnamed x24, local copies, waits for them, and re-layouts  14.3 us
    dot_general x1, matrix products, body(): jnp.dot(hidden, down_full, preferred_element_type=jnp.float32)  13.4 us
    dot_general x1, matrix products, body(): jnp.dot(normed, gate_full, preferred_element_type=jnp.float32) * gate_scale  8.48 us
  transfers between devices with their start and end apart: 6, of which 5 were waited for; matrix products, arithmetic and copies ran while one was open for 8% of the time, Pallas kernels for 0%

profile of v1, /device:TPU:0, one launch (start us, length us, event | category | flops | bytes accessed | tf_op | source)
XLA Modules:
  0.0 376.2 jit_solution(9358879853296601155)
XLA Ops:
  6.5 0.0 all-gather.3.cloned.1.call-start
  6.5 3.1 convert_element_type.29
  9.6 0.0 copy-start
  9.6 0.0 all-gather.3.cloned.1.call-update
  9.6 0.0 all-gather.5.cloned.1.call-start
  9.7 3.2 convert_element_type.30
  12.9 0.0 all-gather.5.cloned.1.call-update
  12.9 0.0 all-reduce.2.cloned.1.call-start
  13.0 0.0 copy-done
  13.0 0.2 convert_element_type.32
  13.2 3.1 collective-permute-start
  16.3 58.6 %collective-permute-done = bf16[1408,512]{1,0:T(8,128)(2,1)S(1)} collective-permute-done((bf16[1408,512]{1,0:T(8,128)(2,1)S(1)}, bf16[1408,512]{1,0:T(8,128)(2,1)S(1)}, u32[]{:S(2)}, u32[]{:S(2)}) %collective-permute-start) | collective-permute-done | bytes 1441824 | tf_op jit(solution)/shard_map/ppermute | solution.py:43
  74.9 0.0 copy-start.1
  74.9 1.1 copy-done.1
  76.0 27.7 %collective-permute-start.1 = (bf16[1408,512]{1,0:T(8,128)(2,1)S(1)}, bf16[1408,512]{1,0:T(8,128)(2,1)}, u32[]{:S(2)}, u32[]{:S(2)}) collective-permute-start(bf16[1408,512]{1,0:T(8,128)(2,1)S(1)} %collective-permute-done), channel_id=1, source_target_pairs={{0,4},{4,8},{8,12},{12,0},{1,5},{5,9},{9,13},{13,1},{2,6},{6,10},{... | collective-permute-start | bytes 4325384 | tf_op jit(solution)/shard_map/ppermute | solution.py:43
  103.8 62.1 %collective-permute-done.1 = bf16[1408,512]{1,0:T(8,128)(2,1)} collective-permute-done((bf16[1408,512]{1,0:T(8,128)(2,1)S(1)}, bf16[1408,512]{1,0:T(8,128)(2,1)}, u32[]{:S(2)}, u32[]{:S(2)}) %collective-permute-start.1) | collective-permute-done | bytes 1441824 | tf_op jit(solution)/shard_map/ppermute | solution.py:43
  165.9 6.4 %collective-permute-start.2 = (bf16[1408,512]{1,0:T(8,128)(2,1)}, bf16[1408,512]{1,0:T(8,128)(2,1)}, u32[]{:S(2)}, u32[]{:S(2)}) collective-permute-start(bf16[1408,512]{1,0:T(8,128)(2,1)} %collective-permute-done.1), channel_id=1, source_target_pairs={{0,4},{4,8},{8,12},{12,0},{1,5},{5,9},{9,13},{13,1},{2,6},{6,10},{... | collective-permute-start | bytes 4325384 | tf_op jit(solution)/shard_map/ppermute | solution.py:43
  172.3 0.0 copy-start.2
  172.3 2.2 fusion.2
  174.5 53.1 %collective-permute-done.2 = bf16[1408,512]{1,0:T(8,128)(2,1)} collective-permute-done((bf16[1408,512]{1,0:T(8,128)(2,1)}, bf16[1408,512]{1,0:T(8,128)(2,1)}, u32[]{:S(2)}, u32[]{:S(2)}) %collective-permute-start.2) | collective-permute-done | bytes 1441824 | tf_op jit(solution)/shard_map/ppermute | solution.py:43
  227.6 2.6 constant_dynamic-update-slice_fusion.7
  230.1 2.6 constant_dynamic-update-slice_fusion.6
  232.8 0.0 copy-done.2
  232.8 1.3 constant_dynamic-update-slice_fusion.5
  234.1 1.3 constant_dynamic-update-slice_fusion.4
  235.4 2.7 constant_dynamic-update-slice_fusion.3
  238.1 2.7 constant_dynamic-update-slice_fusion.2
  240.8 0.0 copy-start.6
  240.8 0.0 copy-start.7
  240.8 1.3 constant_dynamic-update-slice_fusion.1
  242.1 1.4 constant_dynamic-update-slice_fusion
  243.4 0.0 copy-start.3
  243.4 0.0 copy-start.8
  243.4 0.0 all-gather.3.cloned.1.call-done
  243.4 0.0 copy-done.6
  243.5 0.0 copy-done.7
  243.5 8.5 %convolution_multiply_fusion.1 = f32[512,1408]{1,0:T(8,128)} fusion(bf16[2048,1408]{1,0:T(8,128)(2,1)} %all-gather.3.cloned.1.call-done, f32[1408]{0:T(1024)S(1)} %copy-done.6, bf16[512,2048]{1,0:T(8,128)(2,1)} %param.9, f32[2048]{0:T(1024)S(1)} %copy-done.7, f32[512]{0:T(512)S(1)} %add_rsqrt_fusion.1), kind=kOutput, calls=%fused_computation.12 | convolution fusion | flops 2957705216 | bytes 10763776 | tf_op jit(solution)/shard_map/dot_general | solution.py:38
  251.9 0.0 copy-start.4
  251.9 48.0 %all-gather.5.cloned.1.call-done = bf16[2048,1408]{1,0:T(8,128)(2,1)} async-done(((bf16[512,1408]{1,0:T(8,128)(2,1)}), bf16[2048,1408]{1,0:T(8,128)(2,1)}) %all-gather.5.cloned.1.call-update) | async-done | bytes 5767184 | tf_op jit(solution)/shard_map/all_gather | solution.py:36
  300.0 0.0 copy-done.3
  300.0 0.0 copy-done.8
  300.0 13.4 %fusion.7 = bf16[512,2048]{1,0:T(8,128)(2,1)} fusion(bf16[1408,4096]{1,0:T(8,128)(2,1)} %constant_dynamic-update-slice_fusion, s32[]{:T(128)S(6)} %select_n.14, bf16[2048,1408]{1,0:T(8,128)(2,1)} %all-gather.5.cloned.1.call-done, f32[512,1408]{1,0:T(8,128)} %convolution_multiply_fusion.1, f32[1408]{0:T(1024)S(1)} %copy-done.8, ...), kind=kOutput, calls=%fused_computation.14 | convolution fusion | flops 5915869184 | bytes 18628100 | tf_op jit(solution)/shard_map/dot_general | solution.py:47
  313.4 0.0 all-reduce.2.cloned.1.call-update
  313.4 50.5 %all-reduce.2.cloned.1.call-done = bf16[512,2048]{1,0:T(8,128)(2,1)} async-done(((bf16[512,2048]{1,0:T(8,128)(2,1)}), bf16[512,2048]{1,0:T(8,128)(2,1)}) %all-reduce.2.cloned.1.call-update) | async-done | bytes 2097168 | tf_op jit(solution)/shard_map/psum | solution.py:48
  363.9 0.0 copy-done.4
  363.9 2.2 multiply_reduce_fusion
  366.1 0.0 copy-done.5
  366.1 3.6 multiply_convert_fusion
  (3 shorter events, 0.0 us)
Async XLA Ops:
  6.5 236.9 %all-gather.3.cloned.1.call-start = ((), (), s32[]{:S(2)}) async-start(), calls=%async_computation | async-start | bytes 7208960 | tf_op jit(solution)/shard_map/all_gather | solution.py:35
  9.6 3.4 copy-start
  9.6 290.3 %all-gather.5.cloned.1.call-start = ((), (), s32[]{:S(2)}) async-start(), calls=%async_computation.1 | async-start | bytes 7208960 | tf_op jit(solution)/shard_map/all_gather | solution.py:36
  12.9 351.0 %all-reduce.2.cloned.1.call-start = ((), (), s32[]{:S(2)}) async-start(), calls=%async_computation.2 | async-start | bytes 4194304 | tf_op jit(solution)/shard_map/psum | solution.py:48
  13.2 61.8 %collective-permute-start = (bf16[1408,512]{1,0:T(8,128)(2,1)S(1)}, bf16[1408,512]{1,0:T(8,128)(2,1)S(1)}, u32[]{:S(2)}, u32[]{:S(2)}) collective-permute-start(bf16[1408,512]{1,0:T(8,128)(2,1)S(1)} %convert_element_type.32), channel_id=1, source_target_pairs={{0,4},{4,8},{8,12},{12,0},{1,5},{5,9},{9,13},{13,1},{2,6},{6,10},{... | collective-permute-start | bytes 4325384 | tf_op jit(solution)/shard_map/ppermute | solution.py:43
  74.9 1.1 copy-start.1
  76.0 89.9 %collective-permute-start.1 = (bf16[1408,512]{1,0:T(8,128)(2,1)S(1)}, bf16[1408,512]{1,0:T(8,128)(2,1)}, u32[]{:S(2)}, u32[]{:S(2)}) collective-permute-start(bf16[1408,512]{1,0:T(8,128)(2,1)S(1)} %collective-permute-done), channel_id=1, source_target_pairs={{0,4},{4,8},{8,12},{12,0},{1,5},{5,9},{9,13},{13,1},{2,6},{6,10},{... | collective-permute-start | bytes 4325384 | tf_op jit(solution)/shard_map/ppermute | solution.py:43
  165.9 61.6 %collective-permute-start.2 = (bf16[1408,512]{1,0:T(8,128)(2,1)}, bf16[1408,512]{1,0:T(8,128)(2,1)}, u32[]{:S(2)}, u32[]{:S(2)}) collective-permute-start(bf16[1408,512]{1,0:T(8,128)(2,1)} %collective-permute-done.1), channel_id=1, source_target_pairs={{0,4},{4,8},{8,12},{12,0},{1,5},{5,9},{9,13},{13,1},{2,6},{6,10},{... | collective-permute-start | bytes 4325384 | tf_op jit(solution)/shard_map/ppermute | solution.py:43
  172.3 60.5 %copy-start.2 = (bf16[1408,512]{1,0:T(8,128)(2,1)S(1)}, bf16[1408,512]{1,0:T(8,128)(2,1)}, u32[]{:S(2)}) copy-start(bf16[1408,512]{1,0:T(8,128)(2,1)} %copy-done.1) | copy-start | bytes 4325380
  240.8 2.7 copy-start.6
  240.8 2.7 copy-start.7
  243.4 56.5 %copy-start.3 = (bf16[512,2048]{1,0:T(8,128)(2,1)S(1)}, bf16[512,2048]{1,0:T(8,128)(2,1)}, u32[]{:S(2)}) copy-start(bf16[512,2048]{1,0:T(8,128)(2,1)} %param.9) | copy-start | bytes 6291460
  243.4 56.5 %copy-start.8 = (f32[1408]{0:T(1024)S(1)}, f32[1408]{0:T(1024)}, u32[]{:S(2)}) copy-start(f32[1408]{0:T(1024)} %param.14) | copy-start | bytes 16900
  251.9 112.0 %copy-start.4 = (f32[2048]{0:T(1024)S(1)}, f32[2048]{0:T(1024)}, u32[]{:S(2)}) copy-start(f32[2048]{0:T(1024)} %param.16) | copy-start | bytes 24580
  313.4 52.8 %copy-start.5 = (f32[2048]{0:T(1024)S(1)}, f32[2048]{0:T(1024)}, u32[]{:S(2)}) copy-start(f32[2048]{0:T(1024)} %param.17) | copy-start | bytes 24580
Sparse Core Ops, SparseCore 0:
  9.7 164.2 all-gather.2
  175.6 124.2 all-gather.4
  313.5 50.3 all-reduce.1
